TPU v7x, 32 devices: a whole 2x2x4 slice. The times are simulated.
32 devices in a mesh: ep: 4 (over z), tp: 8 (over y, x, core).
Axes of the slice: x: 2, y: 2, z: 4, core: 2. Of those that a mesh axis runs over, the one named last changes fastest.
Arguments:
- tokens: bfloat16 [512, 2048], P('ep', 'tp'), may hold values from -6 to 6
- routes: int32 [512, 2], P('ep'), may hold values from 0 to 3, as said below
- route_weights: float32 [512, 2], P('ep'), may hold values from 0.1 to 1
- grad_out: bfloat16 [512, 2048], P('ep', 'tp'), may hold values from -6 to 6
- w_gate: bfloat16 [4, 2048, 2048], P('ep', 'tp'), may hold values from -0.125 to 0.125
- w_up: bfloat16 [4, 2048, 2048], P('ep', 'tp'), may hold values from -0.125 to 0.125
- w_down: bfloat16 [4, 2048, 2048], P('ep', 'tp')
Outputs:
- grad_tokens: bfloat16 [512, 2048], P('ep', 'tp')
- grad_route: float32 [512, 2], P('ep')
- grad_gate: float32 [4, 2048, 2048], P('ep', 'tp')
- grad_up: float32 [4, 2048, 2048], P('ep', 'tp')
- grad_down: float32 [4, 2048, 2048], P('ep', 'tp')
- gate_row_norms: float32 [4, 2048], P('ep')
- up_row_norms: float32 [4, 2048], P('ep')
- down_row_norms: float32 [4, 2048], P('ep', 'tp')
Inputs may be any that keep to these rules, and one draw needn't show every extreme that they name: `routes`: each token names two different experts of one group: group g holds experts g * 4 to g * 4 + 3. Among the 128 rows of one device along ep no expert is named more than 64 times, and in every draw some expert is named exactly 64 times by the rows of every device along ep.
All inputs are finite; a program needn't handle non-finite values.
Results may differ from a plain program's by a relative error of at most 0.017.
Values may be sent and summed in bfloat16 or wider, within the bound.
A program may use at most 64 MiB of HBM per device.

v0:
```python
import functools

import jax
import jax.numpy as jnp
from jax import lax
from jax.experimental import pallas as pl
from jax.experimental.pallas import tpu as pltpu
from jax.sharding import PartitionSpec as P

MESH = pl.DeviceIdType.MESH
F32 = jnp.float32
BF16 = jnp.bfloat16
NT = (((1,), (1,)), ((), ()))
VMEM = pl.BlockSpec(memory_space=pltpu.VMEM)
ANY = pl.BlockSpec(memory_space=pl.ANY)


def peers(j):
    core, x, y = j % 2, (j // 2) % 2, j // 4
    partner = j + 1 - 2 * core
    xnb = j + 2 - 4 * x
    ynb = j + 4 - 8 * y
    diag = xnb + 4 - 8 * y
    return partner, xnb, ynb, diag


def routing(routes_ref):
    token_count = routes_ref.shape[1]
    r0, r1 = routes_ref[0:1, :], routes_ref[1:2, :]
    eid = lax.broadcasted_iota(jnp.int32, (8, token_count), 0)
    m0, m1 = eid == r0, eid == r1
    m = jnp.logical_or(m0, m1)
    upper = (
        lax.broadcasted_iota(jnp.int32, (token_count, token_count), 0)
        < lax.broadcasted_iota(jnp.int32, (token_count, token_count), 1)
    )
    earlier = jnp.dot(
        jnp.where(m, 1.0, 0.0).astype(BF16),
        jnp.where(upper, 1.0, 0.0).astype(BF16),
        preferred_element_type=F32,
    )
    slot = jnp.where(m, earlier, -1.0)
    return m0, m1, slot


def slot_mask(slot, e, capacity):
    token_count = slot.shape[1]
    ids = lax.broadcasted_iota(jnp.int32, (capacity, token_count), 0).astype(F32)
    return slot[e : e + 1, :] == ids


def signal_all(barrier, devices):
    for device in devices:
        pl.semaphore_signal(barrier, inc=1, device_id=device, device_id_type=MESH)


def remote(src, dst, send_sem, recv_sem, device):
    return pltpu.make_async_remote_copy(
        src_ref=src,
        dst_ref=dst,
        send_sem=send_sem,
        recv_sem=recv_sem,
        device_id=device,
        device_id_type=MESH,
    )


def step_kernel(
    n_ep, n_tp, capacity, routes_ref, weights_ref, tok_ref, go_ref, wg_hbm, wu_hbm, wd_hbm,
    full_hbm, lhs_ref, z_in, route_in, norm_total,
    full, send_buf, wg, wu, wd, back, pair_in, chip_sum, plane_in, z_out,
    part_out, part_in, route_out, norm_out, norm_in,
    in_sem, zs, zr, ts, tr, ps, pr, cs, cr, qs, qr, rs, rr, ns, nr, bs, br,
):
    i, j = lax.axis_index("ep"), lax.axis_index("tp")
    width = tok_ref.shape[1]
    model_width = wg.shape[1]
    n_chip = n_tp // 2
    core = j % 2
    partner, xnb, ynb, diag = peers(j)
    barrier = pltpu.get_barrier_semaphore()
    greet = [(lax.rem(i + d, n_ep), j) for d in range(1, n_ep)]
    greet += [(i, lax.rem(j + d, n_tp)) for d in range(1, n_tp)]
    signal_all(barrier, greet)
    loads = []
    for index, (source, target) in enumerate(((wg_hbm, wg), (wu_hbm, wu), (wd_hbm, wd))):
        load = pltpu.make_async_copy(source, target, in_sem.at[index])
        load.start()
        loads.append(load)

    m0, m1, slot = routing(routes_ref)
    weight = jnp.where(m0, weights_ref[0:1, :], 0.0) + jnp.where(m1, weights_ref[1:2, :], 0.0)
    for e in range(n_ep):
        mask = slot_mask(slot, e, capacity)
        pick = jnp.where(mask, 1.0, 0.0).astype(BF16)
        rows = jnp.dot(pick, tok_ref[...], preferred_element_type=F32)
        grads = jnp.dot(pick, go_ref[...], preferred_element_type=F32)
        scale = jnp.sum(jnp.where(mask, weight[e : e + 1, :], 0.0), axis=1, keepdims=True)
        send_buf[e, 0] = rows.astype(BF16)
        send_buf[e, 1] = (grads * scale).astype(BF16)

    def rows_at(e):
        return pl.ds(pl.multiple_of(e * capacity, capacity), capacity)

    def cols_at(t):
        return pl.ds(pl.multiple_of(t * width, width), width)

    def area(src, col):
        return full.at[:, rows_at(src), cols_at(col)]

    area(i, j)[...] = send_buf[i]
    pl.semaphore_wait(barrier, len(greet))

    z_copies = {}
    for d in [1, 3, 2]:
        e = lax.rem(i + d, n_ep)
        z_copies[d] = remote(send_buf.at[e], area(i, j), zs.at[d], zr.at[d], (e, j))
        z_copies[d].start()

    copies = []
    heard = {}

    def push(kind, d, source, target, device):
        copy = remote(source, target, ts.at[kind, d], tr.at[kind, d], (i, device))
        copy.start()
        copies.append(copy)
        heard[kind, d] = copy

    order = [0, 1, 3, 2]
    for step in range(len(order) + 2):
        if step < len(order):
            d = order[step]
            src = lax.rem(i + n_ep - d, n_ep)
            if d > 0:
                z_copies[d].wait_recv()
            mine = area(src, j) if d > 0 else send_buf.at[i]
            push(0, d, mine, area(src, j), xnb)
            push(1, d, mine, area(src, j), ynb)
            push(4, d, mine, area(src, j), partner)
        if 0 < step <= len(order):
            d = order[step - 1]
            src = lax.rem(i + n_ep - d, n_ep)
            heard[0, d].wait_recv()
            half = full.at[0, rows_at(src), cols_at(xnb)]
            push(2, d, half, half, ynb)
            push(5, d, area(src, xnb), area(src, xnb), partner)
            heard[1, d].wait_recv()
            half = full.at[1, rows_at(src), cols_at(ynb)]
            push(3, d, half, half, xnb)
            push(6, d, area(src, ynb), area(src, ynb), partner)
        if step > 1:
            d = order[step - 2]
            src = lax.rem(i + n_ep - d, n_ep)
            for kind in (0, 1):
                heard[2 + kind, d].wait_recv()
                half = full.at[kind, rows_at(src), cols_at(diag)]
                push(7 + kind, d, half, half, partner)
    for d in order:
        for kind in (4, 5, 6, 7, 8):
            heard[kind, d].wait_recv()

    save = pltpu.make_async_copy(full, full_hbm, in_sem.at[3])
    save.start()
    for load in loads:
        load.wait()
    gate = lax.dot_general(full[0], wg[...], NT, preferred_element_type=F32)
    up = lax.dot_general(full[0], wu[...], NT, preferred_element_type=F32)
    dhid = lax.dot_general(full[1], wd[...], NT, preferred_element_type=F32)
    sig = 1.0 / (1.0 + jnp.exp(-gate))
    active = gate * sig
    slope = sig * (1.0 + gate * (1.0 - sig))
    hidden_f = (active * up).astype(BF16).astype(F32)
    dgate_f = dhid * up * slope
    dup_f = dhid * active
    dgate, dup = dgate_f.astype(BF16), dup_f.astype(BF16)

    ring = [2, 1, 3, 0]
    pair = {}
    for q in range(n_chip):
        cols = slice(2 * q * width, 2 * (q + 1) * width)
        back[:, cols] = (
            jnp.dot(dgate, wg[:, cols], preferred_element_type=F32)
            + jnp.dot(dup, wu[:, cols], preferred_element_type=F32)
        ).astype(BF16)
        for d in ring:
            e = lax.rem(i + d, n_ep)
            pair[d, q] = remote(
                back.at[rows_at(e), cols_at(2 * q + 1 - core)],
                pair_in.at[d, q],
                ps.at[d, q],
                pr.at[d, q],
                (i, partner),
            )
            pair[d, q].start()

    route_terms = hidden_f * dhid
    part_out[...] = jnp.zeros_like(part_out)
    for e in range(n_ep):
        block = route_terms[e * capacity : (e + 1) * capacity, :]
        part_out[e : e + 1, 0:capacity] = jnp.sum(block.T, axis=0, keepdims=True)
    part = []
    for d in range(1, n_tp):
        copy = remote(
            part_out, part_in.at[d - 1], qs.at[d - 1], qr.at[d - 1], (i, lax.rem(j + d, n_tp))
        )
        copy.start()
        part.append(copy)

    plane = {}
    for d in ring:
        e = lax.rem(i + d, n_ep)
        for q in range(n_chip):
            pair[d, q].wait_recv()
            mine = back[rows_at(e), cols_at(2 * q + core)].astype(F32)
            chip_sum[d, q] = (mine + pair_in[d, q].astype(F32)).astype(BF16)
        for kind, target in enumerate((diag, xnb, ynb)):
            plane[d, kind] = remote(
                chip_sum.at[d, target // 2],
                plane_in.at[d, kind],
                cs.at[d, kind],
                cr.at[d, kind],
                (i, target),
            )
            plane[d, kind].start()

    lhs_ref[0] = dgate_f.T.astype(BF16)
    lhs_ref[1] = dup_f.T.astype(BF16)
    lhs_ref[2] = hidden_f.T.astype(BF16)
    rows_norm = model_width // 128
    tile = 512
    for index in range(2):
        for n in range(model_width // tile):
            cols = slice(n * tile, (n + 1) * tile)
            grad = jnp.dot(lhs_ref[index], full[0, :, cols], preferred_element_type=F32)
            norm = jnp.sum(grad * grad, axis=0, keepdims=True)
            for q in range(tile // 128):
                row = index * rows_norm + n * (tile // 128) + q
                norm_out[row : row + 1, :] = norm[:, q * 128 : (q + 1) * 128]
    norms = []
    for d in range(1, n_tp):
        copy = remote(
            norm_out, norm_in.at[d - 1], ns.at[d - 1], nr.at[d - 1], (i, lax.rem(j + d, n_tp))
        )
        copy.start()
        norms.append(copy)

    for copy in part:
        copy.wait_recv()
    total = part_out[...]
    for d in range(1, n_tp):
        total = total + part_in[d - 1]
    route_out[...] = total
    route_in[i] = total
    route = []
    for d in range(1, n_ep):
        copy = remote(
            route_out, route_in.at[i], rs.at[d], rr.at[d], (lax.rem(i + d, n_ep), j)
        )
        copy.start()
        route.append(copy)

    returns = []
    for d in ring:
        for kind in range(3):
            plane[d, kind].wait_recv()
        done = (
            chip_sum[d, j // 2].astype(F32)
            + plane_in[d, 0].astype(F32)
            + plane_in[d, 1].astype(F32)
            + plane_in[d, 2].astype(F32)
        ).astype(BF16)
        if d == 0:
            z_in[i] = done
        else:
            z_out[d] = done
            copy = remote(
                z_out.at[d], z_in.at[i], bs.at[d], br.at[d], (lax.rem(i + d, n_ep), j)
            )
            copy.start()
            returns.append(copy)

    for copy in norms:
        copy.wait_recv()
    total = norm_out[...]
    for d in range(1, n_tp):
        total = total + norm_in[d - 1]
    norm_total[...] = total
    for copy in (*route, *returns):
        copy.wait_recv()
    for copy in (
        *z_copies.values(), *copies, *pair.values(), *part, *plane.values(),
        *norms, *route, *returns,
    ):
        copy.wait_send()
    save.wait()


def finish_kernel(
    n_ep, capacity, routes_ref, weights_ref, full_hbm, lhs_ref, z_in, route_in, norm_total,
    gg_hbm, gu_hbm, gd_hbm, gt_ref, gr_ref, gn_ref, un_ref, dn_ref,
    full, gg, gu, gd, in_sem, out_sem,
):
    loads = []
    for index in range(2):
        load = pltpu.make_async_copy(full_hbm.at[index], full.at[index], in_sem.at[index])
        load.start()
        loads.append(load)
    _, hidden_dev, _ = lhs_ref.shape
    model_width = full.shape[2]
    tile = 512
    stores = []
    down_sums = jnp.zeros((hidden_dev, 128), F32)
    for index, (rhs, buf, out) in enumerate(((0, gg, gg_hbm), (0, gu, gu_hbm), (1, gd, gd_hbm))):
        if index != 1:
            loads[rhs].wait()
        for n in range(model_width // tile):
            cols = slice(n * tile, (n + 1) * tile)
            grad = jnp.dot(lhs_ref[index], full[rhs, :, cols], preferred_element_type=F32)
            buf[:, cols] = grad
            store = pltpu.make_async_copy(
                buf.at[:, cols], out.at[:, cols], out_sem.at[index, n]
            )
            store.start()
            stores.append(store)
            if index == 2:
                square = grad * grad
                for q in range(tile // 128):
                    down_sums = down_sums + square[:, q * 128 : (q + 1) * 128]
    dn_ref[...] = jnp.sum(down_sums.T, axis=0, keepdims=True)
    rows_norm = model_width // 128
    for r in range(rows_norm):
        gn_ref[:, r * 128 : (r + 1) * 128] = norm_total[r : r + 1, :]
        un_ref[:, r * 128 : (r + 1) * 128] = norm_total[rows_norm + r : rows_norm + r + 1, :]

    i = lax.axis_index("ep")
    m0, m1, slot = routing(routes_ref)
    acc = jnp.zeros(gt_ref.shape, F32)
    back_route = []
    for e in range(n_ep):
        pick = jnp.where(slot_mask(slot, e, capacity), 1.0, 0.0)
        acc = acc + jnp.dot(pick.T.astype(BF16), z_in[e], preferred_element_type=F32)
        values = route_in[e, pl.ds(i, 1), :][:, 0:capacity]
        back_route.append(
            jnp.dot(
                values, pick, preferred_element_type=F32, precision=lax.Precision.HIGHEST
            )
        )
    gt_ref[...] = acc.astype(BF16)
    for k, m in enumerate((m0, m1)):
        value = jnp.zeros_like(back_route[0])
        for e in range(n_ep):
            value = value + jnp.where(m[e : e + 1, :], back_route[e], 0.0)
        gr_ref[k : k + 1, :] = value / weights_ref[k : k + 1, :]
    for store in stores:
        store.wait()


def per_device_kernels(tokens, routes, route_weights, grad_out, w_gate, w_up, w_down):
    token_count, width = tokens.shape
    _, hidden_dev, model_width = w_gate.shape
    n_ep, n_tp = lax.axis_size("ep"), lax.axis_size("tp")
    n_chip = n_tp // 2
    capacity = min(3 * token_count // n_ep, token_count // 2)
    rows = n_ep * capacity
    block = (capacity, width)
    norm_rows = 2 * (model_width // 128)
    routes_t, weights_t = routes.T, route_weights.T
    dma = pltpu.SemaphoreType.DMA
    full, lhs, z_in, route_in, norm_total = pl.pallas_call(
        functools.partial(step_kernel, n_ep, n_tp, capacity),
        name="step",
        out_shape=(
            jax.ShapeDtypeStruct((2, rows, model_width), BF16),
            jax.ShapeDtypeStruct((3, hidden_dev, rows), BF16),
            jax.ShapeDtypeStruct((n_ep, *block), BF16),
            jax.ShapeDtypeStruct((n_ep, 8, 128), F32),
            jax.ShapeDtypeStruct((norm_rows, 128), F32),
        ),
        in_specs=[VMEM] * 4 + [ANY] * 3,
        out_specs=(ANY, VMEM, VMEM, VMEM, VMEM),
        scratch_shapes=[
            pltpu.VMEM((2, rows, model_width), BF16),
            pltpu.VMEM((n_ep, 2, *block), BF16),
            *[pltpu.VMEM((hidden_dev, model_width), BF16)] * 3,
            pltpu.VMEM((rows, model_width), BF16),
            pltpu.VMEM((n_ep, n_chip, *block), BF16),
            pltpu.VMEM((n_ep, n_chip, *block), BF16),
            pltpu.VMEM((n_ep, 3, *block), BF16),
            pltpu.VMEM((n_ep, *block), BF16),
            pltpu.VMEM((8, 128), F32),
            pltpu.VMEM((n_tp - 1, 8, 128), F32),
            pltpu.VMEM((8, 128), F32),
            pltpu.VMEM((norm_rows, 128), F32),
            pltpu.VMEM((n_tp - 1, norm_rows, 128), F32),
            dma((4,)),
            *[dma((n_ep,))] * 2,
            *[dma((9, n_ep))] * 2,
            *[dma((n_ep, n_chip))] * 2,
            *[dma((n_ep, 3))] * 2,
            *[dma((n_tp - 1,))] * 2,
            *[dma((n_ep,))] * 2,
            *[dma((n_tp - 1,))] * 2,
            *[dma((n_ep,))] * 2,
        ],
        compiler_params=pltpu.CompilerParams(collective_id=0, has_side_effects=True),
    )(routes_t, weights_t, tokens, grad_out, w_gate[0], w_up[0], w_down[0])

    grad_shape = jax.ShapeDtypeStruct((hidden_dev, model_width), F32)
    norm_shape = jax.ShapeDtypeStruct((1, model_width), F32)
    grad_gate, grad_up, grad_down, grad_tokens, grad_route, gate_norms, up_norms, down_norms = (
        pl.pallas_call(
            functools.partial(finish_kernel, n_ep, capacity),
            name="finish",
            out_shape=(
                *[grad_shape] * 3,
                jax.ShapeDtypeStruct((token_count, width), BF16),
                jax.ShapeDtypeStruct((2, token_count), F32),
                *[norm_shape] * 2,
                jax.ShapeDtypeStruct((1, hidden_dev), F32),
            ),
            in_specs=[VMEM, VMEM, ANY, VMEM, VMEM, VMEM, VMEM],
            out_specs=(*[ANY] * 3, *[VMEM] * 5),
            scratch_shapes=[
                pltpu.VMEM((2, rows, model_width), BF16),
                *[pltpu.VMEM((hidden_dev, model_width), F32)] * 3,
                dma((2,)),
                dma((3, model_width // 512)),
            ],
        )(routes_t, weights_t, full, lhs, z_in, route_in, norm_total)
    )
    return (
        grad_tokens,
        grad_route.T,
        grad_gate[None],
        grad_up[None],
        grad_down[None],
        gate_norms,
        up_norms,
        down_norms,
    )


def silu_parts(pre_act):
    sigmoid_val = jax.nn.sigmoid(pre_act)
    return (pre_act * sigmoid_val, sigmoid_val * (1.0 + pre_act * (1.0 - sigmoid_val)))


def per_device(tokens, routes, route_weights, grad_out, w_gate, w_up, w_down):
    token_count, feature_dev = tokens.shape
    experts_dev, hidden_dev, model_width = w_gate.shape
    ep_size = lax.axis_size("ep")
    expert_total = experts_dev * ep_size
    capacity = min(3 * token_count // expert_total, token_count // 2)
    slot_count = expert_total * capacity
    row_count = ep_size * capacity
    flat_ids = routes.reshape(-1)
    pair_count = flat_ids.shape[0]
    one_hot = (flat_ids[:, None] == jnp.arange(expert_total, dtype=jnp.int32)[None, :]).astype(
        jnp.bfloat16
    )
    lower = (
        jnp.arange(pair_count, dtype=jnp.int32)[:, None]
        > jnp.arange(pair_count, dtype=jnp.int32)[None, :]
    ).astype(jnp.bfloat16)
    earlier = jnp.dot(lower, one_hot, preferred_element_type=jnp.float32)
    slot_ids = jnp.sum(earlier * one_hot.astype(jnp.float32), axis=1).astype(jnp.int32)
    position = flat_ids % experts_dev * row_count + flat_ids // experts_dev * capacity + slot_ids
    dispatch = (position[None, :] == jnp.arange(slot_count, dtype=jnp.int32)[:, None]).astype(
        jnp.bfloat16
    )
    weight_flat = route_weights.reshape(-1)
    token_rows = jnp.repeat(tokens, 2, axis=0)
    scaled = (weight_flat[:, None] * jnp.repeat(grad_out, 2, axis=0).astype(jnp.float32)).astype(
        jnp.bfloat16
    )
    send_shape = (experts_dev, ep_size, capacity, feature_dev)
    x_send = (
        jnp.dot(dispatch, token_rows, preferred_element_type=jnp.float32)
        .astype(jnp.bfloat16)
        .reshape(send_shape)
    )
    s_send = (
        jnp.dot(dispatch, scaled, preferred_element_type=jnp.float32)
        .astype(jnp.bfloat16)
        .reshape(send_shape)
    )
    x_recv, s_recv = (
        lax.all_to_all(x_send, "ep", split_axis=1, concat_axis=1, tiled=True),
        lax.all_to_all(s_send, "ep", split_axis=1, concat_axis=1, tiled=True),
    )
    x_full, s_full = (
        lax.all_gather(x_recv, "tp", axis=3, tiled=True),
        lax.all_gather(s_recv, "tp", axis=3, tiled=True),
    )
    x_rows = x_full.reshape(experts_dev, row_count, model_width)
    s_rows = s_full.reshape(experts_dev, row_count, model_width)
    gate = jnp.einsum("erd,efd->erf", x_rows, w_gate, preferred_element_type=jnp.float32)
    up = jnp.einsum("erd,efd->erf", x_rows, w_up, preferred_element_type=jnp.float32)
    dhid = jnp.einsum("erd,efd->erf", s_rows, w_down, preferred_element_type=jnp.float32)
    active, slope = silu_parts(gate)
    hidden = (active * up).astype(jnp.bfloat16)
    partial_value = jnp.sum(hidden.astype(jnp.float32) * dhid, axis=2)
    dgate = (dhid * up * slope).astype(jnp.bfloat16)
    dup = (dhid * active).astype(jnp.bfloat16)
    grad_gate = jnp.einsum("erf,erd->efd", dgate, x_rows, preferred_element_type=jnp.float32)
    grad_up = jnp.einsum("erf,erd->efd", dup, x_rows, preferred_element_type=jnp.float32)
    grad_down = jnp.einsum("erf,erd->efd", hidden, s_rows, preferred_element_type=jnp.float32)
    back_terms = jnp.einsum("erf,efd->erd", dgate, w_gate, preferred_element_type=jnp.float32)
    back_terms = back_terms + jnp.einsum(
        "erf,efd->erd", dup, w_up, preferred_element_type=jnp.float32
    )
    back_terms = back_terms.reshape(experts_dev, ep_size, capacity, model_width)
    gate_norms = jnp.sum(grad_gate * grad_gate, axis=1)
    up_norms = jnp.sum(grad_up * grad_up, axis=1)
    down_norms = jnp.sum(grad_down * grad_down, axis=2)
    partial_value, gate_norms, up_norms = lax.psum((partial_value, gate_norms, up_norms), "tp")
    partial_sent = partial_value.reshape(experts_dev, ep_size, capacity)
    dtok_mine = lax.psum_scatter(
        back_terms.astype(jnp.bfloat16), "tp", scatter_dimension=3, tiled=True
    ).astype(jnp.float32)
    returned, partial_back = (
        lax.all_to_all(
            dtok_mine.astype(jnp.bfloat16), "ep", split_axis=1, concat_axis=1, tiled=True
        ).astype(dtok_mine.dtype),
        lax.all_to_all(
            partial_sent.astype(jnp.bfloat16), "ep", split_axis=1, concat_axis=1, tiled=True
        ).astype(partial_sent.dtype),
    )
    slot_rows = jnp.take(returned.reshape(slot_count, feature_dev), position, axis=0)
    grad_tokens = jnp.sum(slot_rows.reshape(token_count, 2, feature_dev), axis=1).astype(
        jnp.bfloat16
    )
    slot_partial = jnp.take(partial_back.reshape(slot_count), position, axis=0)
    grad_route = (slot_partial / weight_flat).reshape(token_count, 2)
    return (
        grad_tokens,
        grad_route,
        grad_gate,
        grad_up,
        grad_down,
        gate_norms,
        up_norms,
        down_norms,
    )


def solution(mesh):
    in_specs = (
        P("ep", "tp"),
        P("ep", None),
        P("ep", None),
        P("ep", "tp"),
        P("ep", "tp", None),
        P("ep", "tp", None),
        P("ep", "tp", None),
    )
    out_specs = (
        P("ep", "tp"),
        P("ep", None),
        P("ep", "tp", None),
        P("ep", "tp", None),
        P("ep", "tp", None),
        P("ep", None),
        P("ep", None),
        P("ep", "tp"),
    )
    fits = mesh.shape["tp"] == 8 and mesh.shape["ep"] == 4
    return jax.shard_map(
        per_device_kernels if fits else per_device, mesh=mesh, in_specs=in_specs, out_specs=out_specs, check_vma=False
    )
```

profile of v0, /device:TPU:0, one launch (start us, length us, event | category | flops | bytes accessed | tf_op | source)
XLA Modules:
  0.0 45.3 jit_solution(14958629739026141783)
XLA Ops:
  0.6 38.7 %step.1 = (bf16[2,256,2048]{2,1,0:T(8,128)(2,1)}, bf16[3,256,256]{2,1,0:T(8,128)(2,1)}, bf16[4,64,256]{2,1,0:T(8,128)(2,1)}, f32[4,8,128]{2,1,0:T(8,128)}, f32[32,128]{1,0:T(8,128)}) custom-call(s32[2,128]{1,0:T(2,128)} %bitcast.12, f32[2,128]{1,0:T(2,128)} %bitcast.14, bf16[128,256]{1,0:T(8,128)(2,1)} %tok_ref.1, bf16[128,256]{1,0:T(8,128)(2,1)} %go_ref.1, ...), custom_call_target="tpu_custom_call" | custom-call | tf_op jit(solution)/shard_map/step/pallas_call | solution.py:369
  39.3 6.0 %finish.1 = (f32[256,2048]{1,0:T(8,128)}, f32[256,2048]{1,0:T(8,128)}, f32[256,2048]{1,0:T(8,128)}, bf16[128,256]{1,0:T(8,128)(2,1)}, f32[2,128]{1,0:T(2,128)}, ...) custom-call(s32[2,128]{1,0:T(2,128)} %bitcast.13, f32[2,128]{1,0:T(2,128)} %bitcast.15, ...), custom_call_target="tpu_custom_call" | custom-call | tf_op jit(solution)/shard_map/finish/pallas_call | solution.py:411
where the time goes:
time: 45.5 us; the launch traced here: 45.3 us
  Pallas kernels  44.6 us (98%)
  between operations  0.64 us (1%)
    pallas_call x1, Pallas kernels, per_device_kernels(): pl.pallas_call(functools.partial(step_kernel, n_ep, n_tp, capacity), name...  38.7 us
    pallas_call x1, Pallas kernels, per_device_kernels(): pl.pallas_call(functools.partial(finish_kernel, n_ep, capacity), name='fi...  5.97 us

commit v1 on v0

v1 whole, which is shorter than its diff:
```python
import functools

import jax
import jax.numpy as jnp
from jax import lax
from jax.experimental import pallas as pl
from jax.experimental.pallas import tpu as pltpu
from jax.sharding import PartitionSpec as P

MESH = pl.DeviceIdType.MESH
F32 = jnp.float32
BF16 = jnp.bfloat16
VMEM_LIMIT = 24 * 2**20
DIRECT = (0, 1,)
ORDER = (
    "A0", "W", "A1", "B0", "C0", "A2", "A3", "B1", "C1", "X", "B2n", "B3n",
    "G02", "B2s", "B3s", "C2", "C3", "K02", "F1", "n24", "F0", "E24", "P", "K24",
    "F3", "R1", "F2", "g0", "H1", "g1", "N", "H0", "g2", "N1", "R2", "H3",
    "H2", "N2",
)
NT = (((1,), (1,)), ((), ()))
VMEM = pl.BlockSpec(memory_space=pltpu.VMEM)
ANY = pl.BlockSpec(memory_space=pl.ANY)
HBM = pl.BlockSpec(memory_space=pltpu.HBM)


def peers(j):
    core, x, y = j % 2, (j // 2) % 2, j // 4
    partner = j + 1 - 2 * core
    xnb = j + 2 - 4 * x
    ynb = j + 4 - 8 * y
    diag = xnb + 4 - 8 * y
    return partner, xnb, ynb, diag


def routing(routes_ref):
    token_count = routes_ref.shape[1]
    r0, r1 = routes_ref[0:1, :], routes_ref[1:2, :]
    eid = lax.broadcasted_iota(jnp.int32, (8, token_count), 0)
    m0, m1 = eid == r0, eid == r1
    m = jnp.logical_or(m0, m1)
    upper = (
        lax.broadcasted_iota(jnp.int32, (token_count, token_count), 0)
        < lax.broadcasted_iota(jnp.int32, (token_count, token_count), 1)
    )
    earlier = jnp.dot(
        jnp.where(m, 1.0, 0.0).astype(BF16),
        jnp.where(upper, 1.0, 0.0).astype(BF16),
        preferred_element_type=F32,
    )
    slot = jnp.where(m, earlier, -1.0)
    return m0, m1, slot


def slot_mask(slot, e, capacity):
    token_count = slot.shape[1]
    ids = lax.broadcasted_iota(jnp.int32, (capacity, token_count), 0).astype(F32)
    return slot[e : e + 1, :] == ids


def signal_all(barrier, devices):
    for device in devices:
        pl.semaphore_signal(barrier, inc=1, device_id=device, device_id_type=MESH)


def remote(src, dst, send_sem, recv_sem, device):
    return pltpu.make_async_remote_copy(
        src_ref=src,
        dst_ref=dst,
        send_sem=send_sem,
        recv_sem=recv_sem,
        device_id=device,
        device_id_type=MESH,
    )


def mirrored(side, plane):
    return plane + side * (3 - 2 * plane)


def swapped(near, plane):
    return plane + near * (2 * ((3 - plane) // 3) - (4 - plane) // 3)


def source_of(i, k):
    side = i // 2
    return mirrored(side, swapped(mirrored(side, i), k))


def chunk_of(i, source):
    side = i // 2
    return swapped(mirrored(side, i), mirrored(side, source))


def targets_of(i):
    side = i // 2
    near = mirrored(side, i)
    return [mirrored(side, e) for e in (near + 1, 3 - 3 * near, near + 2)]


def step_kernel(
    n_ep, n_tp, capacity, routes_hbm, weights_hbm, tok_hbm, go_hbm, wg_hbm, wu_hbm, wd_hbm,
    gg, gu, gd, z_in, route_in, norm_total, down_out, routes_ref, weights_ref,
    full, send_buf, tok_ref, go_ref, wgu, wd, w_own, w_peer, acc, mine, lhs_ref, pair_out, pair_in, chip_sum, plane_in,
    z_out, part_out, part_pair, part_sum, part_in, part_z, norm_out, norm_pair, norm_sum, norm_in,
    load_sem, one_send, one_recv, zr, ts, tr, pr, pair_r, plane_r,
):
    i, j = lax.axis_index("ep"), lax.axis_index("tp")
    width = tok_ref.shape[1]
    hidden_dev, model_width = wd.shape
    n_chip = n_tp // 2
    core = j % 2
    partner, xnb, ynb, diag = peers(j)
    barrier = pltpu.get_barrier_semaphore()
    greet = [(lax.rem(i + d, n_ep), j) for d in range(1, n_ep)]
    greet += [(i, device) for device in (partner, xnb, ynb, diag)]
    signal_all(barrier, greet)
    loads = []
    for index, (source, target) in enumerate((
        (routes_hbm, routes_ref), (weights_hbm, weights_ref), (tok_hbm, tok_ref),
        (go_hbm, go_ref), (wg_hbm, wgu.at[0:hidden_dev]),
        (wu_hbm, wgu.at[hidden_dev : 2 * hidden_dev]), (wd_hbm, wd),
    )):
        load = pltpu.make_async_copy(source, target, load_sem.at[index])
        load.start()
        loads.append(load)

    def cols_at(t):
        return pl.ds(pl.multiple_of(t * width, width), width)

    def rows_of(k):
        return slice(k * capacity, (k + 1) * capacity)

    def block(p, k, col):
        return full.at[p, rows_of(k), cols_at(col)]

    for load in loads[:4]:
        load.wait()
    with jax.named_scope("pick"):
        m0, m1, slot = routing(routes_ref)
        weight = jnp.where(m0, weights_ref[0:1, :], 0.0) + jnp.where(m1, weights_ref[1:2, :], 0.0)
        for e in range(n_ep):
            mask = slot_mask(slot, e, capacity)
            pick = jnp.where(mask, 1.0, 0.0).astype(BF16)
            rows = jnp.dot(pick, tok_ref[...], preferred_element_type=F32)
            grads = jnp.dot(pick, go_ref[...], preferred_element_type=F32)
            scale = jnp.sum(jnp.where(mask, weight[e : e + 1, :], 0.0), axis=1, keepdims=True)
            send_buf[e, 0] = rows.astype(BF16)
            send_buf[e, 1] = (grads * scale).astype(BF16)
        full.at[:, rows_of(0), cols_at(j)][...] = send_buf[i]
    with jax.named_scope("barrier"):
        pl.semaphore_wait(barrier, len(greet))

    def z_copy(p, e):
        k = chunk_of(e, i)
        target = full.at[p, pl.ds(pl.multiple_of(k * capacity, capacity), capacity), cols_at(j)]
        return remote(send_buf.at[e, p], target, one_send.at[0], zr.at[k - 1, p], (e, j))

    for e in targets_of(i):
        for p in range(2):
            z_copy(p, e).start()

    def push(k, index, p, col, device, far=0):
        landed = pr.at[k, far] if index is None else tr.at[k, index]
        remote(block(p, k, col), block(p, k, col), ts.at[k], landed, (i, device)).start()

    def heard(k, index, p, col):
        remote(block(p, k, col), block(p, k, col), ts.at[k], tr.at[k, index], (i, xnb)).wait_recv()

    def spread(k):
        with jax.named_scope(f"A{k}"):
            for p in range(2):
                if k > 0:
                    mine = block(p, k, j)
                    remote(mine, mine, one_send.at[0], zr.at[k - 1, p], (i, xnb)).wait_recv()
                push(k, 2 * p, p, j, xnb)
                push(k, 2 * p + 1, p, j, ynb)
                if k in DIRECT:
                    push(k, 4 + p, p, j, diag)
                else:

                    @pl.when(core == 0)
                    def _(p=p):
                        push(k, 4 + p, p, j, diag)

                push(k, None, p, j, partner)

    def forward(k):
        with jax.named_scope(f"B{k}"):
            for p in range(2):
                for index, col, device in ((2 * p, xnb, ynb), (2 * p + 1, ynb, xnb)):
                    heard(k, index, p, col)
                    if k not in DIRECT and index in (0, 3):

                        @pl.when(core == 1)
                        def _(p=p, col=col, device=device):
                            push(k, 4 + p, p, col, device)

                    push(k, None, p, col, partner)

    def relay(k):
        with jax.named_scope(f"C{k}"):
            heard(k, 4, 0, diag)
            push(k, None, 0, diag, partner, 1)
            heard(k, 5, 1, diag)
            push(k, None, 1, diag, partner, 1)

    def relayed(k, far):
        with jax.named_scope(f"D{k}_{far}"):
            half = full.at[:, rows_of(k), 0 : (1 if far else 3) * width]
            remote(half, half, ts.at[k], pr.at[k, far], (i, partner)).wait_recv()

    def products(rows, chip):
        cols = pl.ds(pl.multiple_of(chip * 2 * width, 2 * width), 2 * width)
        return (
            lax.dot_general(full[0, rows, cols], wgu[:, cols], NT, preferred_element_type=F32),
            lax.dot_general(full[1, rows, cols], wd[:, cols], NT, preferred_element_type=F32),
        )

    def start_compute(first, last):
        for k in range(first, last):
            relayed(k, 0)
        with jax.named_scope(f"n{first}_{last}"):
            rows = slice(first * capacity, last * capacity)
            sums = [products(rows, chip // 2) for chip in (j, xnb, ynb)]
            both, dhid = (a + b + c for a, b, c in zip(*sums))
            acc[rows, 0 : 2 * hidden_dev] = both
            acc[rows, 2 * hidden_dev :] = dhid

    def compute(first, last, started=False):
        for k in range(first, last):
            for far in range(1 if started else 0, 2):
                relayed(k, far)
        with jax.named_scope(f"G{first}_{last}"):
            rows = slice(first * capacity, last * capacity)
            if started:
                both, dhid = products(rows, diag // 2)
                both = both + acc[rows, 0 : 2 * hidden_dev]
                dhid = dhid + acc[rows, 2 * hidden_dev :]
            else:
                both = lax.dot_general(full[0, rows, :], wgu[...], NT, preferred_element_type=F32)
                dhid = lax.dot_general(full[1, rows, :], wd[...], NT, preferred_element_type=F32)
            gate, up = both[:, 0:hidden_dev], both[:, hidden_dev:]
            sig = 1.0 / (1.0 + jnp.exp(-gate))
            active = gate * sig
            slope = sig * (1.0 + gate * (1.0 - sig))
            hidden_f = (active * up).astype(BF16).astype(F32)
            dgate_f = dhid * up * slope
            dup_f = dhid * active
            pair = jnp.concatenate([dgate_f.astype(BF16), dup_f.astype(BF16)], axis=1)
            pair_out[rows, :] = pair
            remote(
                pair_out.at[rows], pair_in.at[rows],
                one_send.at[1], pair_r.at[first], (i, partner),
            ).start()
            mine[rows, :] = jnp.dot(pair, w_own[...], preferred_element_type=F32)
            lhs_ref[0, :, rows] = dgate_f.T.astype(BF16)
            lhs_ref[1, :, rows] = dup_f.T.astype(BF16)
            lhs_ref[2, :, rows] = hidden_f.T.astype(BF16)
            terms = hidden_f * dhid
            for k in range(first, last):
                part = terms[(k - first) * capacity : (k - first + 1) * capacity, :]
                part_out[k : k + 1, 0:capacity] = jnp.sum(part.T, axis=0, keepdims=True)

    def finish_compute(first, last):
        with jax.named_scope(f"K{first}_{last}"):
            rows = slice(first * capacity, last * capacity)
            remote(
                pair_in.at[rows], pair_in.at[rows],
                one_send.at[1], pair_r.at[first], (i, partner),
            ).wait_recv()
            total = mine[rows, :] + jnp.dot(
                pair_in[rows, :], w_peer[...], preferred_element_type=F32
            )
            for k in range(first, last):
                part = total[(k - first) * capacity : (k - first + 1) * capacity, :]
                for q in range(n_chip):
                    chip_sum[k, q] = part[:, q * width : (q + 1) * width].astype(BF16)

    def chip_reduce(k):
        with jax.named_scope(f"F{k}"):
            for kind, target in enumerate((diag, xnb, ynb)):
                remote(
                    chip_sum.at[k, target // 2], plane_in.at[k, kind],
                    one_send.at[2], plane_r.at[k], (i, target),
                ).start()

    def plane_reduce(k):
        with jax.named_scope(f"H{k}"):
            remote(
                plane_in.at[k], plane_in.at[k], one_send.at[2], plane_r.at[k], (i, xnb)
            ).wait_recv()
            done = (
                chip_sum[k, j // 2].astype(F32)
                + plane_in[k, 0].astype(F32)
                + plane_in[k, 1].astype(F32)
                + plane_in[k, 2].astype(F32)
            ).astype(BF16)
            if k == 0:
                z_in[i] = done
            else:
                z_out[k - 1] = done
                remote(
                    z_out.at[k - 1], z_in.at[i], one_send.at[3], one_recv.at[0],
                    (source_of(i, k), j),
                ).start()

    def load_weights():
        for load in loads[4:]:
            load.wait()
        for q in range(n_chip):
            block_cols = slice(q * width, (q + 1) * width)
            remote(
                wgu.at[:, cols_at(2 * q + 1 - core)], w_peer.at[:, block_cols],
                one_send.at[9], one_recv.at[6], (i, partner),
            ).start()
            w_own[:, block_cols] = wgu[:, cols_at(2 * q + core)]

    def peer_weights():
        with jax.named_scope("X"):
            remote(w_peer, w_peer, one_send.at[9], one_recv.at[6], (i, partner)).wait_recv()

    part_copy = remote(part_out, part_pair, one_send.at[4], one_recv.at[1], (i, partner))
    norm_copy = remote(norm_out, norm_pair, one_send.at[6], one_recv.at[3], (i, partner))

    def route_chip():
        with jax.named_scope("R1"):
            part_copy.wait_recv()
            part_sum[...] = part_out[...] + part_pair[...]
            for kind, target in enumerate((diag, xnb, ynb)):
                remote(
                    part_sum, part_in.at[kind], one_send.at[5], one_recv.at[2], (i, target)
                ).start()

    def route_plane():
        with jax.named_scope("R2"):
            remote(part_in, part_in, one_send.at[5], one_recv.at[2], (i, xnb)).wait_recv()
            total = part_sum[...] + part_in[0] + part_in[1] + part_in[2]
            part_z[...] = total
            route_in[i] = total
            for d in range(1, n_ep):
                remote(
                    part_z, route_in.at[i], one_send.at[7], one_recv.at[4],
                    (lax.rem(i + d, n_ep), j),
                ).start()

    def norm_chip():
        with jax.named_scope("N1"):
            norm_copy.wait_recv()
            norm_sum[...] = norm_out[...] + norm_pair[...]
            for kind, target in enumerate((diag, xnb, ynb)):
                remote(
                    norm_sum, norm_in.at[kind], one_send.at[8], one_recv.at[5], (i, target)
                ).start()

    def norm_plane():
        with jax.named_scope("N2"):
            remote(norm_in, norm_in, one_send.at[8], one_recv.at[5], (i, xnb)).wait_recv()
            norm_total[...] = norm_sum[...] + norm_in[0] + norm_in[1] + norm_in[2]

    rows_norm = model_width // 128
    tile = 512

    def weight_grad(index, rhs, out):
        with jax.named_scope(f"grad{index}"):
            sums = jnp.zeros((out.shape[0], 128), F32)
            for n in range(model_width // tile):
                cols = slice(n * tile, (n + 1) * tile)
                grad = jnp.dot(lhs_ref[index], full[rhs, :, cols], preferred_element_type=F32)
                out[:, cols] = grad
                square = grad * grad
                if rhs == 0:
                    norm = jnp.sum(square, axis=0, keepdims=True)
                    for q in range(tile // 128):
                        row = index * rows_norm + n * (tile // 128) + q
                        norm_out[row : row + 1, :] = norm[:, q * 128 : (q + 1) * 128]
                else:
                    for q in range(tile // 128):
                        sums = sums + square[:, q * 128 : (q + 1) * 128]
            if rhs == 1:
                down_out[...] = jnp.sum(sums.T, axis=0, keepdims=True)

    part_out[...] = jnp.zeros_like(part_out)
    steps = {
        "A": spread, "B": forward, "C": relay, "F": chip_reduce, "H": plane_reduce,
    }
    others = {
        "W": load_weights,
        "X": peer_weights,
        "P": part_copy.start,
        "R1": route_chip,
        "R2": route_plane,
        "g0": lambda: weight_grad(0, 0, gg),
        "g1": lambda: weight_grad(1, 0, gu),
        "g2": lambda: weight_grad(2, 1, gd),
        "N": norm_copy.start,
        "N1": norm_chip,
        "N2": norm_plane,
    }
    for name in ORDER:
        if name in others:
            others[name]()
        elif name[0] == "K":
            finish_compute(int(name[1]), int(name[2]))
        elif name[0] == "n":
            start_compute(int(name[1]), int(name[2]))
        elif name[0] in "GE":
            compute(int(name[1]), int(name[2]), name[0] == "E")
        else:
            step, k = steps[name[0]], int(name[1])
            if len(name) == 2:
                step(k)
            else:

                @pl.when(core == "sn".index(name[2]))
                def _(step=step, k=k):
                    step(k)

    with jax.named_scope("zret"):
        remote(part_in, part_in, one_send.at[7], one_recv.at[4], (i, xnb)).wait_recv()
        remote(z_out, z_out, one_send.at[3], one_recv.at[0], (i, xnb)).wait_recv()
    with jax.named_scope("drain"):
        part_copy.wait_send()
        norm_copy.wait_send()
        for k in range(n_ep):
            sent = full.at[:, rows_of(k), 0 : 7 * width]
            remote(sent, sent, ts.at[k], pr.at[k, 0], (i, xnb)).wait_send()
        for sent, index in (
            (send_buf.at[0:3], 0), (pair_in, 1), (plane_in, 2), (z_out, 3), (part_in, 5),
            (part_in, 7), (norm_in, 8), (w_peer, 9),
        ):
            remote(sent, sent, one_send.at[index], one_recv.at[0], (i, xnb)).wait_send()


def finish_kernel(
    n_ep, capacity, gg, gu, gd, z_in, route_in, norm_total, down_sums, routes_ref, weights_ref,
    gg_hbm, gu_hbm, gd_hbm, gt_hbm, gr_hbm, gn_hbm, un_hbm, dn_hbm,
    gt_ref, gr_ref, gn_ref, un_ref, out_sem, small_sem,
):
    hidden_dev, model_width = gg.shape
    tile = hidden_dev // out_sem.shape[1]
    stores = []
    for index, (buf, out) in enumerate(((gg, gg_hbm), (gu, gu_hbm), (gd, gd_hbm))):
        for n in range(out_sem.shape[1]):
            rows = slice(n * tile, (n + 1) * tile)
            store = pltpu.make_async_copy(buf.at[rows], out.at[rows], out_sem.at[index, n])
            store.start()
            stores.append(store)

    def save(source, target, index):
        store = pltpu.make_async_copy(source, target, small_sem.at[index])
        store.start()
        stores.append(store)

    save(down_sums, dn_hbm, 0)
    rows_norm = model_width // 128
    for r in range(rows_norm):
        gn_ref[:, r * 128 : (r + 1) * 128] = norm_total[r : r + 1, :]
        un_ref[:, r * 128 : (r + 1) * 128] = norm_total[rows_norm + r : rows_norm + r + 1, :]
    save(gn_ref, gn_hbm, 1)
    save(un_ref, un_hbm, 2)

    i = lax.axis_index("ep")
    m0, m1, slot = routing(routes_ref)
    acc = jnp.zeros(gt_ref.shape, F32)
    back_route = []
    for e in range(n_ep):
        pick = jnp.where(slot_mask(slot, e, capacity), 1.0, 0.0)
        acc = acc + jnp.dot(pick.T.astype(BF16), z_in[e], preferred_element_type=F32)
        values = route_in[e, pl.ds(chunk_of(e, i), 1), :][:, 0:capacity]
        back_route.append(
            jnp.dot(
                values, pick, preferred_element_type=F32, precision=lax.Precision.HIGHEST
            )
        )
    gt_ref[...] = acc.astype(BF16)
    save(gt_ref, gt_hbm, 3)
    for k, m in enumerate((m0, m1)):
        value = jnp.zeros_like(back_route[0])
        for e in range(n_ep):
            value = value + jnp.where(m[e : e + 1, :], back_route[e], 0.0)
        gr_ref[k : k + 1, :] = value / weights_ref[k : k + 1, :]
    save(gr_ref, gr_hbm, 4)
    for store in stores:
        store.wait()


def per_device_kernels(tokens, routes, route_weights, grad_out, w_gate, w_up, w_down):
    token_count, width = tokens.shape
    _, hidden_dev, model_width = w_gate.shape
    n_ep, n_tp = lax.axis_size("ep"), lax.axis_size("tp")
    n_chip = n_tp // 2
    capacity = min(3 * token_count // n_ep, token_count // 2)
    rows = n_ep * capacity
    block = (capacity, width)
    norm_rows = 2 * (model_width // 128)
    dma = pltpu.SemaphoreType.DMA
    part = pltpu.VMEM((8, 128), F32)
    norm = pltpu.VMEM((norm_rows, 128), F32)
    grad = pltpu.VMEM((hidden_dev, model_width), F32)
    inner = pl.pallas_call(
        functools.partial(step_kernel, n_ep, n_tp, capacity),
        name="step",
        out_shape=(
            *[grad] * 3,
            pltpu.VMEM((n_ep, *block), BF16),
            pltpu.VMEM((n_ep, 8, 128), F32),
            norm,
            pltpu.VMEM((1, hidden_dev), F32),
            pltpu.VMEM((2, token_count), jnp.int32),
            pltpu.VMEM((2, token_count), F32),
        ),
        in_specs=[HBM] * 7,
        out_specs=[VMEM] * 9,
        scratch_shapes=[
            pltpu.VMEM((2, rows, model_width), BF16),
            pltpu.VMEM((n_ep, 2, *block), BF16),
            *[pltpu.VMEM((token_count, width), BF16)] * 2,
            pltpu.VMEM((2 * hidden_dev, model_width), BF16),
            pltpu.VMEM((hidden_dev, model_width), BF16),
            *[pltpu.VMEM((2 * hidden_dev, model_width // 2), BF16)] * 2,
            pltpu.VMEM((rows, 3 * hidden_dev), F32),
            pltpu.VMEM((rows, model_width // 2), F32),
            pltpu.VMEM((3, hidden_dev, rows), BF16),
            *[pltpu.VMEM((rows, 2 * hidden_dev), BF16)] * 2,
            pltpu.VMEM((n_ep, n_chip, *block), BF16),
            pltpu.VMEM((n_ep, 3, *block), BF16),
            pltpu.VMEM((n_ep - 1, *block), BF16),
            part, part, part, pltpu.VMEM((3, 8, 128), F32), part,
            norm, norm, norm, pltpu.VMEM((3, norm_rows, 128), F32),
            dma((7,)),
            dma((10,)),
            dma((7,)),
            dma((n_ep - 1, 2)),
            dma((n_ep,)),
            dma((n_ep, 6)),
            dma((n_ep, 2)),
            *[dma((n_ep,))] * 2,
        ],
        compiler_params=pltpu.CompilerParams(
            collective_id=0, has_side_effects=True, vmem_limit_bytes=VMEM_LIMIT
        ),
    )(*[
        pltpu.with_memory_space_constraint(operand, pltpu.HBM)
        for operand in (
            routes.T, route_weights.T, tokens, grad_out, w_gate[0], w_up[0], w_down[0]
        )
    ])

    grad_shape = jax.ShapeDtypeStruct((hidden_dev, model_width), F32)
    norm_shape = jax.ShapeDtypeStruct((1, model_width), F32)
    grad_gate, grad_up, grad_down, grad_tokens, grad_route, gate_norms, up_norms, down_norms = (
        pl.pallas_call(
            functools.partial(finish_kernel, n_ep, capacity),
            name="finish",
            out_shape=(
                *[grad_shape] * 3,
                jax.ShapeDtypeStruct((token_count, width), BF16),
                jax.ShapeDtypeStruct((2, token_count), F32),
                *[norm_shape] * 2,
                jax.ShapeDtypeStruct((1, hidden_dev), F32),
            ),
            in_specs=[VMEM] * 9,
            out_specs=[ANY] * 8,
            scratch_shapes=[
                pltpu.VMEM((token_count, width), BF16),
                pltpu.VMEM((2, token_count), F32),
                *[pltpu.VMEM((1, model_width), F32)] * 2,
                dma((3, 4)),
                dma((5,)),
            ],
            compiler_params=pltpu.CompilerParams(vmem_limit_bytes=VMEM_LIMIT),
        )(*inner)
    )
    return (
        grad_tokens,
        grad_route.T,
        grad_gate[None],
        grad_up[None],
        grad_down[None],
        gate_norms,
        up_norms,
        down_norms,
    )


def silu_parts(pre_act):
    sigmoid_val = jax.nn.sigmoid(pre_act)
    return (pre_act * sigmoid_val, sigmoid_val * (1.0 + pre_act * (1.0 - sigmoid_val)))


def per_device(tokens, routes, route_weights, grad_out, w_gate, w_up, w_down):
    token_count, feature_dev = tokens.shape
    experts_dev, hidden_dev, model_width = w_gate.shape
    ep_size = lax.axis_size("ep")
    expert_total = experts_dev * ep_size
    capacity = min(3 * token_count // expert_total, token_count // 2)
    slot_count = expert_total * capacity
    row_count = ep_size * capacity
    flat_ids = routes.reshape(-1)
    pair_count = flat_ids.shape[0]
    one_hot = (flat_ids[:, None] == jnp.arange(expert_total, dtype=jnp.int32)[None, :]).astype(
        jnp.bfloat16
    )
    lower = (
        jnp.arange(pair_count, dtype=jnp.int32)[:, None]
        > jnp.arange(pair_count, dtype=jnp.int32)[None, :]
    ).astype(jnp.bfloat16)
    earlier = jnp.dot(lower, one_hot, preferred_element_type=jnp.float32)
    slot_ids = jnp.sum(earlier * one_hot.astype(jnp.float32), axis=1).astype(jnp.int32)
    position = flat_ids % experts_dev * row_count + flat_ids // experts_dev * capacity + slot_ids
    dispatch = (position[None, :] == jnp.arange(slot_count, dtype=jnp.int32)[:, None]).astype(
        jnp.bfloat16
    )
    weight_flat = route_weights.reshape(-1)
    token_rows = jnp.repeat(tokens, 2, axis=0)
    scaled = (weight_flat[:, None] * jnp.repeat(grad_out, 2, axis=0).astype(jnp.float32)).astype(
        jnp.bfloat16
    )
    send_shape = (experts_dev, ep_size, capacity, feature_dev)
    x_send = (
        jnp.dot(dispatch, token_rows, preferred_element_type=jnp.float32)
        .astype(jnp.bfloat16)
        .reshape(send_shape)
    )
    s_send = (
        jnp.dot(dispatch, scaled, preferred_element_type=jnp.float32)
        .astype(jnp.bfloat16)
        .reshape(send_shape)
    )
    x_recv, s_recv = (
        lax.all_to_all(x_send, "ep", split_axis=1, concat_axis=1, tiled=True),
        lax.all_to_all(s_send, "ep", split_axis=1, concat_axis=1, tiled=True),
    )
    x_full, s_full = (
        lax.all_gather(x_recv, "tp", axis=3, tiled=True),
        lax.all_gather(s_recv, "tp", axis=3, tiled=True),
    )
    x_rows = x_full.reshape(experts_dev, row_count, model_width)
    s_rows = s_full.reshape(experts_dev, row_count, model_width)
    gate = jnp.einsum("erd,efd->erf", x_rows, w_gate, preferred_element_type=jnp.float32)
    up = jnp.einsum("erd,efd->erf", x_rows, w_up, preferred_element_type=jnp.float32)
    dhid = jnp.einsum("erd,efd->erf", s_rows, w_down, preferred_element_type=jnp.float32)
    active, slope = silu_parts(gate)
    hidden = (active * up).astype(jnp.bfloat16)
    partial_value = jnp.sum(hidden.astype(jnp.float32) * dhid, axis=2)
    dgate = (dhid * up * slope).astype(jnp.bfloat16)
    dup = (dhid * active).astype(jnp.bfloat16)
    grad_gate = jnp.einsum("erf,erd->efd", dgate, x_rows, preferred_element_type=jnp.float32)
    grad_up = jnp.einsum("erf,erd->efd", dup, x_rows, preferred_element_type=jnp.float32)
    grad_down = jnp.einsum("erf,erd->efd", hidden, s_rows, preferred_element_type=jnp.float32)
    back_terms = jnp.einsum("erf,efd->erd", dgate, w_gate, preferred_element_type=jnp.float32)
    back_terms = back_terms + jnp.einsum(
        "erf,efd->erd", dup, w_up, preferred_element_type=jnp.float32
    )
    back_terms = back_terms.reshape(experts_dev, ep_size, capacity, model_width)
    gate_norms = jnp.sum(grad_gate * grad_gate, axis=1)
    up_norms = jnp.sum(grad_up * grad_up, axis=1)
    down_norms = jnp.sum(grad_down * grad_down, axis=2)
    partial_value, gate_norms, up_norms = lax.psum((partial_value, gate_norms, up_norms), "tp")
    partial_sent = partial_value.reshape(experts_dev, ep_size, capacity)
    dtok_mine = lax.psum_scatter(
        back_terms.astype(jnp.bfloat16), "tp", scatter_dimension=3, tiled=True
    ).astype(jnp.float32)
    returned, partial_back = (
        lax.all_to_all(
            dtok_mine.astype(jnp.bfloat16), "ep", split_axis=1, concat_axis=1, tiled=True
        ).astype(dtok_mine.dtype),
        lax.all_to_all(
            partial_sent.astype(jnp.bfloat16), "ep", split_axis=1, concat_axis=1, tiled=True
        ).astype(partial_sent.dtype),
    )
    slot_rows = jnp.take(returned.reshape(slot_count, feature_dev), position, axis=0)
    grad_tokens = jnp.sum(slot_rows.reshape(token_count, 2, feature_dev), axis=1).astype(
        jnp.bfloat16
    )
    slot_partial = jnp.take(partial_back.reshape(slot_count), position, axis=0)
    grad_route = (slot_partial / weight_flat).reshape(token_count, 2)
    return (
        grad_tokens,
        grad_route,
        grad_gate,
        grad_up,
        grad_down,
        gate_norms,
        up_norms,
        down_norms,
    )


def solution(mesh):
    in_specs = (
        P("ep", "tp"),
        P("ep", None),
        P("ep", None),
        P("ep", "tp"),
        P("ep", "tp", None),
        P("ep", "tp", None),
        P("ep", "tp", None),
    )
    out_specs = (
        P("ep", "tp"),
        P("ep", None),
        P("ep", "tp", None),
        P("ep", "tp", None),
        P("ep", "tp", None),
        P("ep", None),
        P("ep", None),
        P("ep", "tp"),
    )
    fits = mesh.shape["tp"] == 8 and mesh.shape["ep"] == 4
    return jax.shard_map(
        per_device_kernels if fits else per_device, mesh=mesh, in_specs=in_specs, out_specs=out_specs, check_vma=False
    )
```

time: 45.5 us -> 35 us (0.77)
  Pallas kernels: 44.6 us -> 34.2 us
    pallas_call x1, Pallas kernels: 38.7 us -> 31.2 us  [per_device_kernels(): pl.pallas_call(functools.partial(step_kernel, n_ep, n_tp, capacity), name...]
    pallas_call x1, Pallas kernels: 5.97 us -> 3.05 us  [per_device_kernels(): pl.pallas_call(functools.partial(finish_kernel, n_ep, capacity), name='fi...]
where the time goes in v1:
time: 35 us; the launch traced here: 34.9 us
  Pallas kernels  34.2 us (98%)
  between operations  0.64 us (2%)
    pallas_call x1, Pallas kernels, per_device_kernels(): pl.pallas_call(functools.partial(step_kernel, n_ep, n_tp, capacity), name...  31.2 us
    pallas_call x1, Pallas kernels, per_device_kernels(): pl.pallas_call(functools.partial(finish_kernel, n_ep, capacity), name='fi...  3.05 us

profile of v1, /device:TPU:0, one launch (start us, length us, event | category | flops | bytes accessed | tf_op | source)
XLA Modules:
  0.0 34.9 jit_solution(12273917959564762246)
XLA Ops:
  0.6 31.2 %step.1 = (f32[256,2048]{1,0:T(8,128)S(1)}, f32[256,2048]{1,0:T(8,128)S(1)}, f32[256,2048]{1,0:T(8,128)S(1)}, bf16[4,64,256]{2,1,0:T(8,128)(2,1)S(1)}, f32[4,8,1...) custom-call(s32[2,128]{1,0:T(2,128)} %bitcast.12, ...), custom_call_target="tpu_custom_call" | custom-call | tf_op jit(solution)/shard_map/step/pallas_call | solution.py:501
  31.8 3.0 %finish.1 = (f32[256,2048]{1,0:T(8,128)}, f32[256,2048]{1,0:T(8,128)}, f32[256,2048]{1,0:T(8,128)}, bf16[128,256]{1,0:T(8,128)(2,1)}, f32[2,128]{1,0:T(2,128)}, ...) custom-call(f32[256,2048]{1,0:T(8,128)S(1)} %get-tuple-element.25.gg, ...), custom_call_target="tpu_custom_call" | custom-call | tf_op jit(solution)/shard_map/finish/pallas_call | solution.py:553
